TPU v7x, 32 devices: a whole 2x2x4 slice. The times are simulated.
32 devices in a mesh: ep: 8 (over z, core), tp: 4 (over y, x).
Axes of the slice: x: 2, y: 2, z: 4, core: 2. Of those that a mesh axis runs over, the one named last changes fastest.
Arguments:
- mixer_rows: bfloat16 [4096, 2048], P('ep', 'tp'), may hold values from -6 to 6
- expert_rows: bfloat16 [4096, 2048], P('ep', 'tp'), may hold values from -6 to 6
- mixer_gain: float32 [2048], replicated, may hold values from 0.1 to 1.9
- pool_scale: float32 [2048], P('tp'), may hold values from 0.1 to 1.9
- w_in: bfloat16 [2048, 2048], P(None, 'tp'), may hold values from -0.125 to 0.125
- w_mix_out: bfloat16 [2048, 2048], P(None, 'tp'), may hold values from -0.125 to 0.125
- expert_gain: float32 [2048], replicated, may hold values from 0.1 to 1.9
- expert_gate: bfloat16 [8, 2048, 2048], P('ep', None, 'tp'), may hold values from -0.125 to 0.125
- expert_up: bfloat16 [8, 2048, 2048], P('ep', None, 'tp'), may hold values from -0.125 to 0.125
- expert_down: bfloat16 [8, 2048, 2048], P('ep', None, 'tp'), may hold values from -0.125 to 0.125
- routes: int32 [4096, 2], P('ep'), may hold values from 0 to 7, all different within a row; in each aligned block of 512 rows (0 to 511, 512 to 1023, ...) at most 192 rows name the same one
- route_weight: float32 [4096, 2], P('ep'), may hold values from 0.1 to 1
Outputs:
- mixer_output: bfloat16 [4096, 2048], P('ep', 'tp')
- expert_output: bfloat16 [4096, 2048], P('ep', 'tp')
Inputs may be any that keep to these rules, and one draw needn't show every extreme that they name: `routes`: each row names 2 different experts. Among the rows of one device (aligned blocks of 512 rows) no expert is named more than 192 times, a bound that some block reaches.
All inputs are finite; a program needn't handle non-finite values.
Results may differ from a plain program's by a relative error of at most 0.0071.
Values may be sent and summed in bfloat16 or wider, within the bound.
A program may use at most 64 MiB of HBM per device.

v0:
```python
import functools

import jax
import jax.numpy as jnp
from jax import lax
from jax.experimental import pallas as pl
from jax.experimental.pallas import tpu as pltpu
from jax.sharding import PartitionSpec as P

TOP = 2
norm_eps = 1e-05
pool_windows = (2, 4, 8, 16)
RIM = 16
MESH = pl.DeviceIdType.MESH
f32 = jnp.float32
bf16 = jnp.bfloat16


def fused(
    ep,
    tp,
    xm_in,
    xe_in,
    gain_m,
    gain_e,
    scale,
    route_rows,
    rw_rows,
    w_in_h,
    w_mix_h,
    gate_h,
    up_h,
    down_h,
    out_m,
    out_e,
    w_in,
    w_mix,
    gate,
    up,
    down,
    xm,
    normed,
    block,
    disp_send,
    slots,
    hid,
    pooled,
    back_send,
    back_recv,
    ext,
    rim_send,
    rim_recv,
    acc,
    as_rows,
    as_cols,
    w_sem,
    sl_s,
    sl_r,
    xm_s,
    xm_r,
    dp_s,
    dp_r,
    rim_s,
    rim_r,
    po_s,
    po_r,
    hi_s,
    hi_r,
    bk_s,
    bk_r,
):
    me_ep = lax.axis_index("ep")
    me_tp = lax.axis_index("tp")
    rows, feat = xm_in.shape
    cap = slots.shape[2]
    chan = out_m.shape[1]
    width = feat * tp
    chunk = min(rows, 128)

    barrier = pltpu.get_barrier_semaphore()
    for d in range(1, tp):
        pl.semaphore_signal(
            barrier, inc=1, device_id={"tp": lax.rem(me_tp + d, tp)}, device_id_type=MESH
        )
    for d in range(1, ep):
        pl.semaphore_signal(
            barrier, inc=1, device_id={"ep": lax.rem(me_ep + d, ep)}, device_id_type=MESH
        )
    pl.semaphore_wait(barrier, tp + ep - 2)

    def tp_copy(ref, s, r, peer):
        return pltpu.make_async_remote_copy(
            src_ref=ref,
            dst_ref=ref,
            send_sem=s,
            recv_sem=r,
            device_id={"tp": peer},
            device_id_type=MESH,
        )

    def ep_copy(src, dst, s, r, d):
        return pltpu.make_async_remote_copy(
            src_ref=src,
            dst_ref=dst,
            send_sem=s,
            recv_sem=r,
            device_id={"ep": lax.rem(me_ep + d, ep)},
            device_id_type=MESH,
        )

    relayed = tp == 4
    col = lax.rem(me_tp, 2)
    row = me_tp // 2
    beside = row * 2 + (1 - col)
    above = (1 - row) * 2 + col
    across = (1 - row) * 2 + (1 - col)

    def send(slot, s, r):
        if relayed:
            tp_copy(slot(me_tp), s(0), r(0), beside).start()
            tp_copy(slot(me_tp), s(1), r(1), above).start()
        else:
            for d in range(1, tp):
                tp_copy(slot(me_tp), s(d - 1), r(d - 1), lax.rem(me_tp + d, tp)).start()

    def relay(slot, s, r, turn):
        if relayed:
            tp_copy(slot(beside), s(0), r(0), beside).wait_recv()
            tp_copy(slot(above), s(1), r(1), above).wait_recv()
            source = (1 - turn) * beside + turn * above
            peer = (1 - turn) * above + turn * beside
            tp_copy(slot(source), s(2), r(2), peer).start()

    def finish(slot, s, r):
        if relayed:
            tp_copy(slot(across), s(2), r(2), across).wait_recv()
        else:
            for d in range(1, tp):
                p = lax.rem(me_tp - d + tp, tp)
                tp_copy(slot(p), s(d - 1), r(d - 1), p).wait_recv()

    def drain(slot, s, r):
        for d in range(1, tp):
            tp_copy(slot(me_tp), s(d - 1), r(d - 1), lax.rem(me_tp + d, tp)).wait_send()

    def mixer_part():
        return lambda p: xm.at[p], lambda j: xm_s.at[j], lambda j: xm_r.at[j]

    def pooled_part():
        return lambda p: pooled.at[p], lambda j: po_s.at[j], lambda j: po_r.at[j]

    def slot_part(k):
        q = ep_from(k)
        return lambda p: slots.at[q, p], lambda j: sl_s.at[k, j], lambda j: sl_r.at[k, j]

    def hidden_part(k):
        q = ep_from(k)
        return lambda p: hid.at[q, p], lambda j: hi_s.at[k, j], lambda j: hi_r.at[k, j]

    def ep_from(d):
        return lax.rem(me_ep - d + ep, ep)

    xm_load = pltpu.make_async_copy(xm_in, xm.at[me_tp], w_sem.at[5])
    xm_load.start()
    xm_load.wait()
    send(*mixer_part())

    loads = [
        pltpu.make_async_copy(h, v, w_sem.at[i])
        for i, (h, v) in enumerate(
            ((w_in_h, w_in), (gate_h, gate), (up_h, up), (w_mix_h, w_mix), (down_h, down))
        )
    ]
    for load in loads:
        load.start()

    t0 = lax.broadcasted_iota(jnp.int32, (rows, rows), 0)
    t1 = lax.broadcasted_iota(jnp.int32, (rows, rows), 1)
    names = lax.broadcasted_iota(jnp.int32, (ep, rows), 0)
    named = [jnp.where(route_rows[j : j + 1, :] == names, 1.0, 0.0) for j in range(TOP)]
    ahead = jnp.dot(
        sum(named).astype(bf16),
        jnp.where(t0 < t1, 1.0, 0.0).astype(bf16),
        preferred_element_type=f32,
    )
    trow = [
        route_rows[j : j + 1, :] * cap
        + jnp.sum(named[j] * ahead, axis=0, keepdims=True).astype(jnp.int32)
        for j in range(TOP)
    ]
    as_rows[...] = jnp.zeros_like(as_rows)
    for j in range(TOP):
        as_rows[j : j + 1, :] = trow[j].astype(f32)
        as_rows[TOP + j : TOP + j + 1, :] = rw_rows[j : j + 1, :]
    as_cols[...] = as_rows[...].T

    def picked_rows(e):
        slot = lax.broadcasted_iota(jnp.int32, (cap, rows), 0) + e * cap
        hit = (slot == trow[0]) | (slot == trow[1])
        pick = jnp.where(hit, 1.0, 0.0).astype(bf16)
        return jnp.dot(pick, xe_in[...], preferred_element_type=f32).astype(bf16)

    def send_rows(d, carry):
        e = lax.rem(me_ep + d, ep)
        disp_send[e] = picked_rows(e)
        ep_copy(disp_send.at[e], slots.at[me_ep, me_tp], dp_s.at[d], dp_r.at[d], d).start()
        return carry

    lax.fori_loop(1, ep, send_rows, 0)
    slots[me_ep, me_tp] = picked_rows(me_ep)
    relay(*mixer_part(), 0)

    def arrive(k):
        q = ep_from(k)
        ep_copy(disp_send.at[q], slots.at[q, me_tp], dp_s.at[k], dp_r.at[k], k).wait_recv()
        send(*slot_part(k))

    arrive(1)

    def pass_slots(k, carry):
        arrive(k)
        relay(*slot_part(k - 1), lax.rem(k, 2))
        return carry

    early = ep // 2
    lax.fori_loop(2, early, pass_slots, 0)

    def norm_rows(parts, gain):
        parts = [v.astype(f32) for v in parts]
        mean = sum(jnp.sum(v, axis=-1, keepdims=True) for v in parts) / width
        parts = [v - mean for v in parts]
        spread = sum(jnp.sum(v * v, axis=-1, keepdims=True) for v in parts) / width
        inv = lax.rsqrt(spread + norm_eps)
        return [
            (v * inv * gain[:, p * feat : (p + 1) * feat]).astype(bf16)
            for p, v in enumerate(parts)
        ]

    finish(*mixer_part())
    loads[0].wait()

    def project(i, carry):
        at = pl.ds(pl.multiple_of(i * chunk, chunk), chunk)
        for p, v in enumerate(norm_rows([xm[p, at, :] for p in range(tp)], gain_m)):
            normed[:, p * feat : (p + 1) * feat] = v
        inner = jnp.dot(normed[...], w_in[...], preferred_element_type=f32).astype(bf16)
        ext[pl.ds(pl.multiple_of(RIM + i * chunk, RIM), chunk), :] = inner.astype(f32)
        return carry

    lax.fori_loop(0, rows // chunk, project, 0)
    rim_send[0] = ext[rows : rows + RIM, :].astype(bf16)
    rim_send[1] = ext[RIM : 2 * RIM, :].astype(bf16)
    up_rim = ep_copy(rim_send.at[0], rim_recv.at[0], rim_s.at[0], rim_r.at[0], 1)
    down_rim = ep_copy(rim_send.at[1], rim_recv.at[1], rim_s.at[1], rim_r.at[1], ep - 1)
    up_rim.start()
    down_rim.start()

    lax.fori_loop(early, ep - 1, pass_slots, 0)

    up_rim.wait_recv()
    down_rim.wait_recv()
    low = rim_recv[0].astype(f32)
    high = rim_recv[1].astype(f32)
    ext[0:RIM, :] = jnp.where(me_ep > 0, low, 0.0)
    ext[RIM + rows : 2 * RIM + rows, :] = jnp.where(me_ep < ep - 1, high, 0.0)

    group_width = chan * tp // len(pool_windows)
    channel = me_tp * chan + lax.broadcasted_iota(jnp.int32, (1, chan), 1)
    seq_len = rows * ep
    for i in range(rows // chunk):
        first = RIM + i * chunk
        position = me_ep * rows + i * chunk + lax.broadcasted_iota(jnp.int32, (chunk, 1), 0)
        running = jnp.zeros((chunk, chan), f32)
        result = jnp.zeros((chunk, chan), f32)
        last = 0
        for g, window in enumerate(pool_windows):
            half = window // 2
            for o in list(range(-half, -last)) + list(range(last, half)):
                running = running + ext[first + o : first + o + chunk, :]
            last = half
            lower = jnp.maximum(position - half, 0)
            upper = jnp.minimum(position + half, seq_len)
            counts = (upper - lower).astype(f32)
            member = (channel >= g * group_width) & (channel < (g + 1) * group_width)
            result = jnp.where(member, running / counts, result)
        values = ext[first : first + chunk, :]
        pooled[me_tp, i * chunk : (i + 1) * chunk, :] = (
            (result - values) * scale[...]
        ).astype(bf16)
    send(*pooled_part())
    pass_slots(ep - 1, 0)
    send(*slot_part(0))

    loads[1].wait()
    loads[2].wait()

    def hidden_step(k):
        q = ep_from(k)
        finish(*slot_part(k))
        for p, v in enumerate(norm_rows([slots[q, p] for p in range(tp)], gain_e)):
            block[:, p * feat : (p + 1) * feat] = v
        x = block[...]
        g = jnp.dot(x, gate[...], preferred_element_type=f32)
        u = jnp.dot(x, up[...], preferred_element_type=f32)
        hid[q, me_tp] = (g / (1.0 + jnp.exp(-g)) * u).astype(bf16)
        send(*hidden_part(k))

    units = hid.shape[3]

    def value_step(k):
        q = ep_from(k)
        finish(*hidden_part(k))
        total = jnp.zeros((cap, out_e.shape[1]), f32)
        for p in range(tp):
            total = total + jnp.dot(
                hid[q, p],
                down[p * units : (p + 1) * units, :],
                preferred_element_type=f32,
            )
        return total.astype(bf16)

    def send_value(k):
        q = ep_from(k)
        back_send[q] = value_step(k)
        ep_copy(back_send.at[q], back_recv.at[me_ep], bk_s.at[k], bk_r.at[k], ep - k).start()

    hidden_step(1)
    relay(*slot_part(ep - 1), ep % 2)
    hidden_step(2)
    relay(*slot_part(0), 1 - ep % 2)
    relay(*pooled_part(), 1)
    relay(*hidden_part(1), 0)

    loads[3].wait()
    finish(*pooled_part())

    def mix_out(i, carry):
        at = pl.ds(pl.multiple_of(i * chunk, chunk), chunk)
        total = jnp.zeros((chunk, chan), f32)
        for p in range(tp):
            total = total + jnp.dot(
                pooled[p, at, :],
                w_mix[p * chan : (p + 1) * chan, :],
                preferred_element_type=f32,
            )
        out_m[at, :] = total.astype(bf16)
        return carry

    lax.fori_loop(0, rows // chunk, mix_out, 0)
    loads[4].wait()

    def expert(k, carry):
        hidden_step(k)
        relay(*hidden_part(k - 1), lax.rem(k, 2))
        send_value(k - 2)
        return carry

    lax.fori_loop(3, ep, expert, 0)
    hidden_step(0)
    relay(*hidden_part(ep - 1), ep % 2)
    send_value(ep - 2)
    relay(*hidden_part(0), 1 - ep % 2)
    send_value(ep - 1)

    def combine(e):
        slot = lax.broadcasted_iota(jnp.int32, (rows, cap), 1) + e * cap
        weight = jnp.zeros((rows, cap), f32)
        for j in range(TOP):
            own_slot = as_cols[:, j : j + 1].astype(jnp.int32)
            weight = weight + jnp.where(slot == own_slot, as_cols[:, TOP + j : TOP + j + 1], 0.0)
        coarse = weight.astype(bf16)
        fine = (weight - coarse.astype(f32)).astype(bf16)
        v = back_recv[e]
        return jnp.dot(coarse, v, preferred_element_type=f32) + jnp.dot(
            fine, v, preferred_element_type=f32
        )

    acc[...] = jnp.zeros_like(acc)

    def gather_value(k, carry):
        e = lax.rem(me_ep + k, ep)
        ep_copy(back_send.at[e], back_recv.at[e], bk_s.at[k], bk_r.at[k], k).wait_recv()
        acc[...] += combine(e)
        return carry

    lax.fori_loop(1, ep - 2, gather_value, 0)
    back_recv[me_ep] = value_step(0)
    acc[...] += combine(me_ep)
    lax.fori_loop(ep - 2, ep, gather_value, 0)
    out_e[...] = acc[...].astype(bf16)

    drain(*mixer_part())
    drain(*pooled_part())
    up_rim.wait_send()
    down_rim.wait_send()

    def drain_ep(k, carry):
        e = lax.rem(me_ep + k, ep)
        q = ep_from(k)
        ep_copy(disp_send.at[e], slots.at[me_ep, me_tp], dp_s.at[k], dp_r.at[k], k).wait_send()
        ep_copy(back_send.at[q], back_recv.at[me_ep], bk_s.at[k], bk_r.at[k], ep - k).wait_send()
        return carry

    lax.fori_loop(1, ep, drain_ep, 0)

    def drain_tp(k, carry):
        drain(*slot_part(k))
        drain(*hidden_part(k))
        return carry

    lax.fori_loop(0, ep, drain_tp, 0)


def on_device(
    mixer_rows,
    expert_rows,
    mixer_gain,
    pool_scale,
    w_in,
    w_mix_out,
    expert_gain,
    expert_gate,
    expert_up,
    expert_down,
    routes,
    route_weight,
    *,
    ep,
    tp,
):
    rows, feat = mixer_rows.shape
    width = feat * tp
    cap = (3 * TOP * rows + 2 * ep - 1) // (2 * ep)
    chan = w_in.shape[1]
    units = expert_gate.shape[2]
    vmem = pl.BlockSpec(memory_space=pltpu.VMEM)
    hbm = pl.BlockSpec(memory_space=pl.ANY)
    dma = pltpu.SemaphoreType.DMA
    return pl.pallas_call(
        functools.partial(fused, ep, tp),
        out_shape=(
            jax.ShapeDtypeStruct((rows, w_mix_out.shape[1]), bf16),
            jax.ShapeDtypeStruct((rows, expert_down.shape[2]), bf16),
        ),
        in_specs=[vmem] * 7 + [hbm] * 5,
        out_specs=(vmem, vmem),
        scratch_shapes=[
            pltpu.VMEM(w_in.shape, bf16),
            pltpu.VMEM(w_mix_out.shape, bf16),
            pltpu.VMEM(expert_gate.shape[1:], bf16),
            pltpu.VMEM(expert_up.shape[1:], bf16),
            pltpu.VMEM(expert_down.shape[1:], bf16),
            pltpu.VMEM((tp, rows, feat), bf16),
            pltpu.VMEM((min(rows, 128), width), bf16),
            pltpu.VMEM((cap, width), bf16),
            pltpu.VMEM((ep, cap, feat), bf16),
            pltpu.VMEM((ep, tp, cap, feat), bf16),
            pltpu.VMEM((ep, tp, cap, units), bf16),
            pltpu.VMEM((tp, rows, chan), bf16),
            pltpu.VMEM((ep, cap, expert_down.shape[2]), bf16),
            pltpu.VMEM((ep, cap, expert_down.shape[2]), bf16),
            pltpu.VMEM((rows + 2 * RIM, chan), f32),
            pltpu.VMEM((2, RIM, chan), bf16),
            pltpu.VMEM((2, RIM, chan), bf16),
            pltpu.VMEM((rows, expert_down.shape[2]), f32),
            pltpu.VMEM((8, rows), f32),
            pltpu.VMEM((rows, 8), f32),
            dma((6,)),
            dma((ep, tp - 1)),
            dma((ep, tp - 1)),
            dma((tp - 1,)),
            dma((tp - 1,)),
            dma((ep,)),
            dma((ep,)),
            dma((2,)),
            dma((2,)),
            dma((tp - 1,)),
            dma((tp - 1,)),
            dma((ep, tp - 1)),
            dma((ep, tp - 1)),
            dma((ep,)),
            dma((ep,)),
        ],
        compiler_params=pltpu.CompilerParams(
            collective_id=0, has_side_effects=True, vmem_limit_bytes=62 * 1024 * 1024
        ),
    )(
        mixer_rows,
        expert_rows,
        mixer_gain.reshape(1, width),
        expert_gain.reshape(1, width),
        pool_scale.reshape(1, chan),
        routes.T,
        route_weight.T,
        w_in,
        w_mix_out,
        expert_gate.reshape(expert_gate.shape[1:]),
        expert_up.reshape(expert_up.shape[1:]),
        expert_down.reshape(expert_down.shape[1:]),
    )


def solution(mesh):
    return jax.shard_map(
        functools.partial(on_device, ep=mesh.shape["ep"], tp=mesh.shape["tp"]),
        mesh=mesh,
        in_specs=(
            P("ep", "tp"),
            P("ep", "tp"),
            P(),
            P("tp"),
            P(None, "tp"),
            P(None, "tp"),
            P(),
            P("ep", None, "tp"),
            P("ep", None, "tp"),
            P("ep", None, "tp"),
            P("ep", None),
            P("ep", None),
        ),
        out_specs=(P("ep", "tp"), P("ep", "tp")),
        check_vma=False,
    )
```

profile of v0, /device:TPU:0, one launch (start us, length us, event | category | flops | bytes accessed | tf_op | source)
XLA Modules:
  0.0 170.5 jit_solution(731890658768766045)
XLA Ops:
  0.6 166.2 %shard_map.131 = (bf16[512,512]{1,0:T(8,128)(2,1)}, bf16[512,512]{1,0:T(8,128)(2,1)}) custom-call(bf16[512,512]{1,0:T(8,128)(2,1)} %xm_in.1, bf16[512,512]{1,0:T(8,128)(2,1)} %xe_in.1, f32[1,2048]{1,0:T(1,128)} %bitcast.11, f32[1,2048]{1,0:T(1,128)} %bitcast.12, f32[1,512]{1,0:T(1,128)} %bitcast.15, s32[2,512]{1,0:T(2,128)} %bitcast.13, f32[2,512]{1,0:T(2,128)} %bitcast.14, ...), custom_call_target="tpu_custom_call" | custom-call | tf_op jit(solution)/shard_map/pallas_call | solution.py:439
  166.8 1.9 %copy.16 = bf16[512,512]{1,0:T(8,128)(2,1)} copy(bf16[512,512]{1,0:T(8,128)(2,1)} %get-tuple-element.4) | data formatting | bytes 1048576
  168.7 1.9 %copy.17 = bf16[512,512]{1,0:T(8,128)(2,1)} copy(bf16[512,512]{1,0:T(8,128)(2,1)} %get-tuple-element.5) | data formatting | bytes 1048576
where the time goes:
time: 171 us
  Pallas kernels  166 us (97%)
  local copies, waits for them, and re-layouts  3.74 us (2%)
    pallas_call x1, Pallas kernels, on_device(): pl.pallas_call(functools.partial(fused, ep, tp), out_shape=(jax.ShapeDtyp...  166 us
    unnamed x2, local copies, waits for them, and re-layouts  3.74 us

commit v1 on v0

--- a/solution.py
+++ b/solution.py
@@ -11,6 +11,9 @@
 norm_eps = 1e-05
 pool_windows = (2, 4, 8, 16)
 RIM = 16
+AHEAD = 3
+BEHIND = 3
+POOL_AT = 7
 MESH = pl.DeviceIdType.MESH
 f32 = jnp.float32
 bf16 = jnp.bfloat16
@@ -411,6 +414,480 @@
     lax.fori_loop(0, ep, drain_tp, 0)
 
 
+def square(
+    ep,
+    tp,
+    xm_in,
+    xe_in,
+    gain_m,
+    gain_e,
+    scale,
+    route_rows,
+    rw_rows,
+    w_in_h,
+    w_mix_h,
+    gate_h,
+    up_h,
+    down_h,
+    out_m,
+    out_e,
+    w_in,
+    w_mix,
+    gate,
+    up,
+    down,
+    xm,
+    normed,
+    block,
+    disp_send,
+    slots,
+    hid,
+    pooled,
+    back_send,
+    back_recv,
+    ext,
+    rim_send,
+    rim_recv,
+    acc,
+    fin_send,
+    fin_recv,
+    as_rows,
+    as_cols,
+    w_sem,
+    sl_s,
+    sl_r,
+    xm_s,
+    xm_r,
+    dp_s,
+    dp_r,
+    rim_s,
+    rim_r,
+    po_s,
+    po_r,
+    hi_s,
+    hi_r,
+    bk_s,
+    bk_r,
+    dn_s,
+    dn_r,
+    fi_s,
+    fi_r,
+):
+    me_ep = lax.axis_index("ep")
+    me_tp = lax.axis_index("tp")
+    rows, feat = xe_in.shape
+    cap = slots.shape[2]
+    chan = out_m.shape[1]
+    units = hid.shape[3]
+    cols = out_e.shape[1]
+    width = feat * tp
+    chunk = min(rows, 128)
+
+    col = lax.rem(me_tp, 2)
+    row = me_tp // 2
+    beside = row * 2 + (1 - col)
+    above = (1 - row) * 2 + col
+    across = (1 - row) * 2 + (1 - col)
+
+    barrier = pltpu.get_barrier_semaphore()
+    for d in range(1, tp):
+        pl.semaphore_signal(
+            barrier, inc=1, device_id={"tp": lax.rem(me_tp + d, tp)}, device_id_type=MESH
+        )
+    for d in range(1, ep):
+        pl.semaphore_signal(
+            barrier, inc=1, device_id={"ep": lax.rem(me_ep + d, ep)}, device_id_type=MESH
+        )
+
+    xm_load = pltpu.make_async_copy(xm_in, xm.at[me_tp], w_sem.at[0])
+    xm_load.start()
+
+    def unit_rows(r, c):
+        return pl.ds(pl.multiple_of((r * 2 + c) * units, units), units)
+
+    loads = [
+        pltpu.make_async_copy(h, v, w_sem.at[i + 1])
+        for i, (h, v) in enumerate(
+            (
+                (w_in_h, w_in),
+                (gate_h, gate),
+                (up_h, up),
+                (w_mix_h, w_mix),
+                (down_h.at[unit_rows(0, col), :], down.at[col, 0]),
+                (down_h.at[unit_rows(1, col), :], down.at[col, 1]),
+            )
+        )
+    ]
+    for load in loads:
+        load.start()
+
+    def tp_copy(src, dst, s, r, peer):
+        return pltpu.make_async_remote_copy(
+            src_ref=src,
+            dst_ref=dst,
+            send_sem=s,
+            recv_sem=r,
+            device_id={"tp": peer},
+            device_id_type=MESH,
+        )
+
+    def ep_copy(src, dst, s, r, d):
+        return pltpu.make_async_remote_copy(
+            src_ref=src,
+            dst_ref=dst,
+            send_sem=s,
+            recv_sem=r,
+            device_id={"ep": lax.rem(me_ep + d, ep)},
+            device_id_type=MESH,
+        )
+
+    def send(slot, s, r):
+        mine = slot(me_tp)
+        tp_copy(mine, mine, s(0), r(0), beside).start()
+        tp_copy(mine, mine, s(1), r(1), above).start()
+
+    def relay(slot, s, r, turn):
+        tp_copy(slot(beside), slot(beside), s(0), r(0), beside).wait_recv()
+        tp_copy(slot(above), slot(above), s(1), r(1), above).wait_recv()
+        source = slot((1 - turn) * beside + turn * above)
+        tp_copy(source, source, s(2), r(2), (1 - turn) * above + turn * beside).start()
+
+    def finish(slot, s, r):
+        tp_copy(slot(across), slot(across), s(2), r(2), across).wait_recv()
+
+    def drain(slot, s, r):
+        mine = slot(me_tp)
+        for j in range(3):
+            tp_copy(mine, mine, s(j), r(j), beside).wait_send()
+
+    def mixer_part():
+        return lambda p: xm.at[p], lambda j: xm_s.at[j], lambda j: xm_r.at[j]
+
+    def pooled_part():
+        return lambda p: pooled.at[p], lambda j: po_s.at[j], lambda j: po_r.at[j]
+
+    def ep_from(d):
+        return lax.rem(me_ep - d + ep, ep)
+
+    def slot_part(k):
+        q = ep_from(k)
+        return lambda p: slots.at[q, p], lambda j: sl_s.at[k, j], lambda j: sl_r.at[k, j]
+
+    def hidden_copy(k, part):
+        ref = hid.at[ep_from(k), part]
+        return tp_copy(ref, ref, hi_s.at[k], hi_r.at[k], above)
+
+    def down_copy(r):
+        return tp_copy(
+            down_h.at[unit_rows(r, 1 - col), :], down.at[col, r], dn_s.at[r], dn_r.at[r], beside
+        )
+
+    t0 = lax.broadcasted_iota(jnp.int32, (rows, rows), 0)
+    t1 = lax.broadcasted_iota(jnp.int32, (rows, rows), 1)
+    names = lax.broadcasted_iota(jnp.int32, (ep, rows), 0)
+    named = [jnp.where(route_rows[j : j + 1, :] == names, 1.0, 0.0) for j in range(TOP)]
+    ahead = jnp.dot(
+        sum(named).astype(bf16),
+        jnp.where(t0 < t1, 1.0, 0.0).astype(bf16),
+        preferred_element_type=f32,
+    )
+    trow = [
+        route_rows[j : j + 1, :] * cap
+        + jnp.sum(named[j] * ahead, axis=0, keepdims=True).astype(jnp.int32)
+        for j in range(TOP)
+    ]
+    as_rows[...] = jnp.zeros_like(as_rows)
+    for j in range(TOP):
+        as_rows[j : j + 1, :] = trow[j].astype(f32)
+        as_rows[TOP + j : TOP + j + 1, :] = rw_rows[j : j + 1, :]
+    as_cols[...] = as_rows[...].T
+
+    xm_load.wait()
+    pl.semaphore_wait(barrier, tp + ep - 2)
+    send(*mixer_part())
+
+    def picked_rows(e):
+        slot = lax.broadcasted_iota(jnp.int32, (cap, rows), 0) + e * cap
+        hit = (slot == trow[0]) | (slot == trow[1])
+        pick = jnp.where(hit, 1.0, 0.0).astype(bf16)
+        return jnp.dot(pick, xe_in[...], preferred_element_type=f32).astype(bf16)
+
+    def send_rows(d, carry):
+        e = lax.rem(me_ep + d, ep)
+        disp_send[e] = picked_rows(e)
+        ep_copy(disp_send.at[e], slots.at[me_ep, me_tp], dp_s.at[d], dp_r.at[d], d).start()
+        return carry
+
+    lax.fori_loop(1, ep, send_rows, 0)
+    slots[me_ep, me_tp] = picked_rows(me_ep)
+    down_copy(0).start()
+
+    def arrive(k):
+        q = ep_from(k)
+        ep_copy(disp_send.at[q], slots.at[q, me_tp], dp_s.at[k], dp_r.at[k], k).wait_recv()
+        send(*slot_part(k))
+
+    arrive(1)
+    down_copy(1).start()
+    relay(*mixer_part(), 0)
+    for k in range(2, AHEAD + 1):
+        arrive(k)
+
+    def norm_rows(parts, gain):
+        parts = [v.astype(f32) for v in parts]
+        mean = sum(jnp.sum(v, axis=-1, keepdims=True) for v in parts) / width
+        parts = [v - mean for v in parts]
+        spread = sum(jnp.sum(v * v, axis=-1, keepdims=True) for v in parts) / width
+        inv = lax.rsqrt(spread + norm_eps)
+        return [
+            (v * inv * gain[:, p * feat : (p + 1) * feat]).astype(bf16)
+            for p, v in enumerate(parts)
+        ]
+
+    relay(*slot_part(1), 0)
+    finish(*mixer_part())
+    loads[0].wait()
+
+    def project(i, carry):
+        at = pl.ds(pl.multiple_of(i * chunk, chunk), chunk)
+        for p, v in enumerate(norm_rows([xm[p, at, :] for p in range(tp)], gain_m)):
+            normed[:, p * feat : (p + 1) * feat] = v
+        inner = jnp.dot(normed[...], w_in[...], preferred_element_type=f32).astype(bf16)
+        ext[pl.ds(pl.multiple_of(RIM + i * chunk, RIM), chunk), :] = inner.astype(f32)
+        return carry
+
+    lax.fori_loop(0, rows // chunk, project, 0)
+    rim_send[0] = ext[rows : rows + RIM, :].astype(bf16)
+    rim_send[1] = ext[RIM : 2 * RIM, :].astype(bf16)
+    up_rim = ep_copy(rim_send.at[0], rim_recv.at[0], rim_s.at[0], rim_r.at[0], 1)
+    down_rim = ep_copy(rim_send.at[1], rim_recv.at[1], rim_s.at[1], rim_r.at[1], ep - 1)
+    up_rim.start()
+    down_rim.start()
+    for load in loads[1:]:
+        load.wait()
+
+    def hidden_step(k):
+        q = ep_from(k)
+        finish(*slot_part(k))
+        for p, v in enumerate(norm_rows([slots[q, p] for p in range(tp)], gain_e)):
+            block[:, p * feat : (p + 1) * feat] = v
+        x = block[...]
+        g = jnp.dot(x, gate[...], preferred_element_type=f32)
+        u = jnp.dot(x, up[...], preferred_element_type=f32)
+        hid[q, row] = (g / (1.0 + jnp.exp(-g)) * u).astype(bf16)
+        hidden_copy(k, row).start()
+
+    def value_step(k):
+        q = ep_from(k)
+        hidden_copy(k, 1 - row).wait_recv()
+        return [
+            (
+                jnp.dot(hid[q, 0], down[c, 0], preferred_element_type=f32)
+                + jnp.dot(hid[q, 1], down[c, 1], preferred_element_type=f32)
+            ).astype(bf16)
+            for c in range(2)
+        ]
+
+    def send_value(k):
+        q = ep_from(k)
+        for c, v in enumerate(value_step(k)):
+            back_send[q, c] = v
+        ep_copy(back_send.at[q], back_recv.at[me_ep], bk_s.at[k], bk_r.at[k], ep - k).start()
+
+    def combine(e):
+        slot = lax.broadcasted_iota(jnp.int32, (rows, cap), 1) + e * cap
+        weight = jnp.zeros((rows, cap), f32)
+        for j in range(TOP):
+            own_slot = as_cols[:, j : j + 1].astype(jnp.int32)
+            weight = weight + jnp.where(slot == own_slot, as_cols[:, TOP + j : TOP + j + 1], 0.0)
+        coarse = weight.astype(bf16)
+        fine = (weight - coarse.astype(f32)).astype(bf16)
+        for c in range(2):
+            v = back_recv[e, c]
+            acc[c] += jnp.dot(coarse, v, preferred_element_type=f32) + jnp.dot(
+                fine, v, preferred_element_type=f32
+            )
+
+    def gather_value(k):
+        e = lax.rem(me_ep + k, ep)
+        ep_copy(back_send.at[e], back_recv.at[e], bk_s.at[k], bk_r.at[k], k).wait_recv()
+        combine(e)
+
+    def pool():
+        up_rim.wait_recv()
+        down_rim.wait_recv()
+        low = rim_recv[0].astype(f32)
+        high = rim_recv[1].astype(f32)
+        ext[0:RIM, :] = jnp.where(me_ep > 0, low, 0.0)
+        ext[RIM + rows : 2 * RIM + rows, :] = jnp.where(me_ep < ep - 1, high, 0.0)
+        group_width = chan * tp // len(pool_windows)
+        channel = me_tp * chan + lax.broadcasted_iota(jnp.int32, (1, chan), 1)
+        seq_len = rows * ep
+        for i in range(rows // chunk):
+            first = RIM + i * chunk
+            position = me_ep * rows + i * chunk + lax.broadcasted_iota(jnp.int32, (chunk, 1), 0)
+            running = jnp.zeros((chunk, chan), f32)
+            result = jnp.zeros((chunk, chan), f32)
+            last = 0
+            for g, window in enumerate(pool_windows):
+                half = window // 2
+                for o in list(range(-half, -last)) + list(range(last, half)):
+                    running = running + ext[first + o : first + o + chunk, :]
+                last = half
+                lower = jnp.maximum(position - half, 0)
+                upper = jnp.minimum(position + half, seq_len)
+                counts = (upper - lower).astype(f32)
+                member = (channel >= g * group_width) & (channel < (g + 1) * group_width)
+                result = jnp.where(member, running / counts, result)
+            values = ext[first : first + chunk, :]
+            pooled[me_tp, i * chunk : (i + 1) * chunk, :] = (
+                (result - values) * scale[...]
+            ).astype(bf16)
+        send(*pooled_part())
+
+    acc[...] = jnp.zeros_like(acc)
+
+    def step(i, carry):
+        @pl.when(i + AHEAD + 1 < ep)
+        def _():
+            arrive(lax.rem(i + AHEAD + 1, ep))
+
+        @pl.when(i + AHEAD + 1 == ep)
+        def _():
+            send(*slot_part(0))
+
+        @pl.when(i + 1 < ep)
+        def _():
+            relay(*slot_part(lax.rem(i + 2, ep)), 1)
+
+        hidden_step(lax.rem(i + 1, ep))
+
+        @pl.when(i == POOL_AT)
+        def _():
+            pool()
+
+        @pl.when(i == 0)
+        def _():
+            for r in range(2):
+                down_copy(r).wait_recv()
+
+        @pl.when(i > 0)
+        def _():
+            send_value(i)
+
+        @pl.when(i > BEHIND)
+        def _():
+            gather_value(i - BEHIND)
+
+        return carry
+
+    lax.fori_loop(0, ep, step, 0)
+    relay(*pooled_part(), 0)
+    for c, v in enumerate(value_step(0)):
+        back_recv[me_ep, c] = v
+    combine(me_ep)
+
+    def rest(k, carry):
+        gather_value(k)
+        return carry
+
+    lax.fori_loop(ep - BEHIND, ep, rest, 0)
+    fin_send[...] = acc[1 - col].astype(bf16)
+    final = tp_copy(fin_send, fin_recv, fi_s.at[0], fi_r.at[0], beside)
+    final.start()
+
+    finish(*pooled_part())
+
+    def mix_out(i, carry):
+        at = pl.ds(pl.multiple_of(i * chunk, chunk), chunk)
+        total = jnp.zeros((chunk, chan), f32)
+        for p in range(tp):
+            total = total + jnp.dot(
+                pooled[p, at, :],
+                w_mix[p * chan : (p + 1) * chan, :],
+                preferred_element_type=f32,
+            )
+        out_m[at, :] = total.astype(bf16)
+        return carry
+
+    lax.fori_loop(0, rows // chunk, mix_out, 0)
+    final.wait_recv()
+    out_e[...] = (acc[col] + fin_recv[...].astype(f32)).astype(bf16)
+
+    final.wait_send()
+    drain(*mixer_part())
+    drain(*pooled_part())
+    up_rim.wait_send()
+    down_rim.wait_send()
+    for r in range(2):
+        down_copy(r).wait_send()
+
+    def drain_ep(k, carry):
+        e = lax.rem(me_ep + k, ep)
+        q = ep_from(k)
+        ep_copy(disp_send.at[e], slots.at[me_ep, me_tp], dp_s.at[k], dp_r.at[k], k).wait_send()
+        ep_copy(back_send.at[q], back_recv.at[me_ep], bk_s.at[k], bk_r.at[k], ep - k).wait_send()
+        return carry
+
+    lax.fori_loop(1, ep, drain_ep, 0)
+
+    def drain_tp(k, carry):
+        drain(*slot_part(k))
+        hidden_copy(k, row).wait_send()
+        return carry
+
+    lax.fori_loop(0, ep, drain_tp, 0)
+
+
+def square_scratch(ep, tp, rows, feat, cap, chan, units, cols, shapes):
+    dma = pltpu.SemaphoreType.DMA
+    width = feat * tp
+    w_in, w_mix, gate, up = shapes
+    return [
+        pltpu.VMEM(w_in, bf16),
+        pltpu.VMEM(w_mix, bf16),
+        pltpu.VMEM(gate, bf16),
+        pltpu.VMEM(up, bf16),
+        pltpu.VMEM((2, 2, units, cols), bf16),
+        pltpu.VMEM((tp, rows, feat), bf16),
+        pltpu.VMEM((min(rows, 128), width), bf16),
+        pltpu.VMEM((cap, width), bf16),
+        pltpu.VMEM((ep, cap, feat), bf16),
+        pltpu.VMEM((ep, tp, cap, feat), bf16),
+        pltpu.VMEM((ep, 2, cap, units), bf16),
+        pltpu.VMEM((tp, rows, chan), bf16),
+        pltpu.VMEM((ep, 2, cap, cols), bf16),
+        pltpu.VMEM((ep, 2, cap, cols), bf16),
+        pltpu.VMEM((rows + 2 * RIM, chan), f32),
+        pltpu.VMEM((2, RIM, chan), bf16),
+        pltpu.VMEM((2, RIM, chan), bf16),
+        pltpu.VMEM((2, rows, cols), f32),
+        pltpu.VMEM((rows, cols), bf16),
+        pltpu.VMEM((rows, cols), bf16),
+        pltpu.VMEM((8, rows), f32),
+        pltpu.VMEM((rows, 8), f32),
+        dma((7,)),
+        dma((ep, 3)),
+        dma((ep, 3)),
+        dma((3,)),
+        dma((3,)),
+        dma((ep,)),
+        dma((ep,)),
+        dma((2,)),
+        dma((2,)),
+        dma((3,)),
+        dma((3,)),
+        dma((ep,)),
+        dma((ep,)),
+        dma((ep,)),
+        dma((ep,)),
+        dma((2,)),
+        dma((2,)),
+        dma((1,)),
+        dma((1,)),
+    ]
+
+
 def on_device(
     mixer_rows,
     expert_rows,
@@ -436,51 +913,57 @@
     vmem = pl.BlockSpec(memory_space=pltpu.VMEM)
     hbm = pl.BlockSpec(memory_space=pl.ANY)
     dma = pltpu.SemaphoreType.DMA
+    square_ok = tp == 4 and ep > AHEAD + 1
+    whole_scratch = [
+        pltpu.VMEM(w_in.shape, bf16),
+        pltpu.VMEM(w_mix_out.shape, bf16),
+        pltpu.VMEM(expert_gate.shape[1:], bf16),
+        pltpu.VMEM(expert_up.shape[1:], bf16),
+        pltpu.VMEM(expert_down.shape[1:], bf16),
+        pltpu.VMEM((tp, rows, feat), bf16),
+        pltpu.VMEM((min(rows, 128), width), bf16),
+        pltpu.VMEM((cap, width), bf16),
+        pltpu.VMEM((ep, cap, feat), bf16),
+        pltpu.VMEM((ep, tp, cap, feat), bf16),
+        pltpu.VMEM((ep, tp, cap, units), bf16),
+        pltpu.VMEM((tp, rows, chan), bf16),
+        pltpu.VMEM((ep, cap, expert_down.shape[2]), bf16),
+        pltpu.VMEM((ep, cap, expert_down.shape[2]), bf16),
+        pltpu.VMEM((rows + 2 * RIM, chan), f32),
+        pltpu.VMEM((2, RIM, chan), bf16),
+        pltpu.VMEM((2, RIM, chan), bf16),
+        pltpu.VMEM((rows, expert_down.shape[2]), f32),
+        pltpu.VMEM((8, rows), f32),
+        pltpu.VMEM((rows, 8), f32),
+        dma((6,)),
+        dma((ep, tp - 1)),
+        dma((ep, tp - 1)),
+        dma((tp - 1,)),
+        dma((tp - 1,)),
+        dma((ep,)),
+        dma((ep,)),
+        dma((2,)),
+        dma((2,)),
+        dma((tp - 1,)),
+        dma((tp - 1,)),
+        dma((ep, tp - 1)),
+        dma((ep, tp - 1)),
+        dma((ep,)),
+        dma((ep,)),
+    ]
+    if square_ok:
+        shapes = (w_in.shape, w_mix_out.shape, expert_gate.shape[1:], expert_up.shape[1:])
+        cols = expert_down.shape[2]
+        whole_scratch = square_scratch(ep, tp, rows, feat, cap, chan, units, cols, shapes)
     return pl.pallas_call(
-        functools.partial(fused, ep, tp),
+        functools.partial(square if square_ok else fused, ep, tp),
         out_shape=(
             jax.ShapeDtypeStruct((rows, w_mix_out.shape[1]), bf16),
             jax.ShapeDtypeStruct((rows, expert_down.shape[2]), bf16),
         ),
-        in_specs=[vmem] * 7 + [hbm] * 5,
+        in_specs=[hbm if square_ok else vmem] + [vmem] * 6 + [hbm] * 5,
         out_specs=(vmem, vmem),
-        scratch_shapes=[
-            pltpu.VMEM(w_in.shape, bf16),
-            pltpu.VMEM(w_mix_out.shape, bf16),
-            pltpu.VMEM(expert_gate.shape[1:], bf16),
-            pltpu.VMEM(expert_up.shape[1:], bf16),
-            pltpu.VMEM(expert_down.shape[1:], bf16),
-            pltpu.VMEM((tp, rows, feat), bf16),
-            pltpu.VMEM((min(rows, 128), width), bf16),
-            pltpu.VMEM((cap, width), bf16),
-            pltpu.VMEM((ep, cap, feat), bf16),
-            pltpu.VMEM((ep, tp, cap, feat), bf16),
-            pltpu.VMEM((ep, tp, cap, units), bf16),
-            pltpu.VMEM((tp, rows, chan), bf16),
-            pltpu.VMEM((ep, cap, expert_down.shape[2]), bf16),
-            pltpu.VMEM((ep, cap, expert_down.shape[2]), bf16),
-            pltpu.VMEM((rows + 2 * RIM, chan), f32),
-            pltpu.VMEM((2, RIM, chan), bf16),
-            pltpu.VMEM((2, RIM, chan), bf16),
-            pltpu.VMEM((rows, expert_down.shape[2]), f32),
-            pltpu.VMEM((8, rows), f32),
-            pltpu.VMEM((rows, 8), f32),
-            dma((6,)),
-            dma((ep, tp - 1)),
-            dma((ep, tp - 1)),
-            dma((tp - 1,)),
-            dma((tp - 1,)),
-            dma((ep,)),
-            dma((ep,)),
-            dma((2,)),
-            dma((2,)),
-            dma((tp - 1,)),
-            dma((tp - 1,)),
-            dma((ep, tp - 1)),
-            dma((ep, tp - 1)),
-            dma((ep,)),
-            dma((ep,)),
-        ],
+        scratch_shapes=whole_scratch,
         compiler_params=pltpu.CompilerParams(
             collective_id=0, has_side_effects=True, vmem_limit_bytes=62 * 1024 * 1024
         ),

time: 171 us -> 160 us (0.936)
  Pallas kernels: 166 us -> 156 us
    pallas_call x1, Pallas kernels: 166 us -> 156 us  [on_device(): pl.pallas_call(functools.partial(square if square_ok else fused, ep, tp),...]
where the time goes in v1:
time: 160 us
  Pallas kernels  156 us (98%)
  local copies, waits for them, and re-layouts  3.74 us (2%)
    pallas_call x1, Pallas kernels, on_device(): pl.pallas_call(functools.partial(square if square_ok else fused, ep, tp),...  156 us
    unnamed x2, local copies, waits for them, and re-layouts  3.74 us

profile of v1, /device:TPU:0, one launch (start us, length us, event | category | flops | bytes accessed | tf_op | source)
XLA Modules:
  0.0 160.1 jit_solution(11249135830059496922)
XLA Ops:
  0.6 155.7 %shard_map.131 = (bf16[512,512]{1,0:T(8,128)(2,1)}, bf16[512,512]{1,0:T(8,128)(2,1)}) custom-call(bf16[512,512]{1,0:T(8,128)(2,1)} %xm_in.1, bf16[512,512]{1,0:T(8,128)(2,1)} %xe_in.1, f32[1,2048]{1,0:T(1,128)} %bitcast.11, f32[1,2048]{1,0:T(1,128)} %bitcast.12, f32[1,512]{1,0:T(1,128)} %bitcast.15, s32[2,512]{1,0:T(2,128)} %bitcast.13, f32[2,512]{1,0:T(2,128)} %bitcast.14, ...), custom_call_target="tpu_custom_call" | custom-call | tf_op jit(solution)/shard_map/pallas_call | solution.py:958
  156.4 1.9 %copy.16 = bf16[512,512]{1,0:T(8,128)(2,1)} copy(bf16[512,512]{1,0:T(8,128)(2,1)} %get-tuple-element.4) | data formatting | bytes 1048576
  158.2 1.9 %copy.17 = bf16[512,512]{1,0:T(8,128)(2,1)} copy(bf16[512,512]{1,0:T(8,128)(2,1)} %get-tuple-element.5) | data formatting | bytes 1048576

commit v2 on v1

--- a/solution.py
+++ b/solution.py
@@ -11,9 +11,28 @@
 norm_eps = 1e-05
 pool_windows = (2, 4, 8, 16)
 RIM = 16
-AHEAD = 3
-BEHIND = 3
-POOL_AT = 7
+ORDER = (
+    ("W", 1), ("XMY", 1), ("P", -1), ("XMY", 0), ("W", 2), ("A", 6),
+    ("W", 3), ("A", 2), ("A", 7), ("W", 0), ("R", 6), ("R", 2),
+    ("R", 7), ("H", 6), ("A", 3), ("A", 1), ("H", 7), ("R", 3),
+    ("H", 2), ("V", 6), ("A", 4), ("H", 3), ("R", 1), ("XMX", 1),
+    ("V", 7), ("V", 2), ("R", 4), ("A", 5), ("XMX", 0), ("H", 4),
+    ("A", 0), ("V", 3), ("R", 5), ("RXM", 1), ("V", 4), ("H", 1),
+    ("R", 0), ("G", 6), ("RXM", 0), ("H", 5), ("V", 1), ("ENT", -1),
+    ("H", 0), ("POOL", -1), ("V", 5), ("V", 0), ("G", 3), ("G", 7),
+    ("G", 0), ("G", 1), ("G", 2), ("G", 4), ("RPO", 0), ("G", 5),
+    ("RPO", 1), ("EX", -1), ("MIX", 0), ("MIX", 1),
+)
+SENDS = (
+    6, 2, 7, 3, 4, 1, 5,
+)
+OVER_X = (
+    ("R", 0), ("R", 3), ("R", 4), ("R", 5), ("R", 7), ("RXM", 1),
+)
+PLACES = (
+    "ENT", "XMY", "W", "R", "G", "RXM", "A", "RPO",
+    "XMX", "H", "EX", "POOL", "MIX", "V",
+)
 MESH = pl.DeviceIdType.MESH
 f32 = jnp.float32
 bf16 = jnp.bfloat16
@@ -505,6 +524,8 @@
     def unit_rows(r, c):
         return pl.ds(pl.multiple_of((r * 2 + c) * units, units), units)
 
+    piece = units // 2
+
     loads = [
         pltpu.make_async_copy(h, v, w_sem.at[i + 1])
         for i, (h, v) in enumerate(
@@ -560,11 +581,16 @@
         for j in range(3):
             tp_copy(mine, mine, s(j), r(j), beside).wait_send()
 
-    def mixer_part():
-        return lambda p: xm.at[p], lambda j: xm_s.at[j], lambda j: xm_r.at[j]
-
-    def pooled_part():
-        return lambda p: pooled.at[p], lambda j: po_s.at[j], lambda j: po_r.at[j]
+    def half_rows(h):
+        return pl.ds(pl.multiple_of(h * (rows // 2), rows // 2), rows // 2)
+
+    def mixer_part(h):
+        at = half_rows(h)
+        return lambda p: xm.at[p, at], lambda j: xm_s.at[h, j], lambda j: xm_r.at[h, j]
+
+    def pooled_part(h):
+        at = half_rows(h)
+        return lambda p: pooled.at[p, at], lambda j: po_s.at[h, j], lambda j: po_r.at[h, j]
 
     def ep_from(d):
         return lax.rem(me_ep - d + ep, ep)
@@ -577,10 +603,24 @@
         ref = hid.at[ep_from(k), part]
         return tp_copy(ref, ref, hi_s.at[k], hi_r.at[k], above)
 
-    def down_copy(r):
+    def down_copy(i):
+        r, part = i // 2, i % 2
+        first = (r * 2 + 1 - col) * units + part * piece
         return tp_copy(
-            down_h.at[unit_rows(r, 1 - col), :], down.at[col, r], dn_s.at[r], dn_r.at[r], beside
-        )
+            down_h.at[pl.ds(pl.multiple_of(first, piece), piece), :],
+            down.at[col, r, pl.ds(pl.multiple_of(part * piece, piece), piece)],
+            dn_s.at[i],
+            dn_r.at[i],
+            beside,
+        )
+
+    def mixer_x(h):
+        slot, s, r = mixer_part(h)
+        tp_copy(slot(me_tp), slot(me_tp), s(0), r(0), beside).start()
+
+    def mixer_y(h):
+        slot, s, r = mixer_part(h)
+        tp_copy(slot(me_tp), slot(me_tp), s(1), r(1), above).start()
 
     t0 = lax.broadcasted_iota(jnp.int32, (rows, rows), 0)
     t1 = lax.broadcasted_iota(jnp.int32, (rows, rows), 1)
@@ -604,7 +644,14 @@
 
     xm_load.wait()
     pl.semaphore_wait(barrier, tp + ep - 2)
-    send(*mixer_part())
+    starts = {
+        "W": lambda k: down_copy(k).start(),
+        "XMX": mixer_x,
+        "XMY": mixer_y,
+    }
+    picks_at = ORDER.index(("P", -1))
+    for op, k in ORDER[:picks_at]:
+        starts[op](k)
 
     def picked_rows(e):
         slot = lax.broadcasted_iota(jnp.int32, (cap, rows), 0) + e * cap
@@ -612,26 +659,23 @@
         pick = jnp.where(hit, 1.0, 0.0).astype(bf16)
         return jnp.dot(pick, xe_in[...], preferred_element_type=f32).astype(bf16)
 
-    def send_rows(d, carry):
+    def send_rows(n, carry):
+        d = sum(jnp.where(n == i, k, 0) for i, k in enumerate(SENDS))
         e = lax.rem(me_ep + d, ep)
         disp_send[e] = picked_rows(e)
         ep_copy(disp_send.at[e], slots.at[me_ep, me_tp], dp_s.at[d], dp_r.at[d], d).start()
         return carry
 
-    lax.fori_loop(1, ep, send_rows, 0)
+    lax.fori_loop(0, ep - 1, send_rows, 0)
     slots[me_ep, me_tp] = picked_rows(me_ep)
-    down_copy(0).start()
 
     def arrive(k):
-        q = ep_from(k)
-        ep_copy(disp_send.at[q], slots.at[q, me_tp], dp_s.at[k], dp_r.at[k], k).wait_recv()
+        @pl.when(k > 0)
+        def _():
+            q = ep_from(k)
+            ep_copy(disp_send.at[q], slots.at[q, me_tp], dp_s.at[k], dp_r.at[k], k).wait_recv()
+
         send(*slot_part(k))
-
-    arrive(1)
-    down_copy(1).start()
-    relay(*mixer_part(), 0)
-    for k in range(2, AHEAD + 1):
-        arrive(k)
 
     def norm_rows(parts, gain):
         parts = [v.astype(f32) for v in parts]
@@ -644,10 +688,6 @@
             for p, v in enumerate(parts)
         ]
 
-    relay(*slot_part(1), 0)
-    finish(*mixer_part())
-    loads[0].wait()
-
     def project(i, carry):
         at = pl.ds(pl.multiple_of(i * chunk, chunk), chunk)
         for p, v in enumerate(norm_rows([xm[p, at, :] for p in range(tp)], gain_m)):
@@ -656,14 +696,19 @@
         ext[pl.ds(pl.multiple_of(RIM + i * chunk, RIM), chunk), :] = inner.astype(f32)
         return carry
 
-    lax.fori_loop(0, rows // chunk, project, 0)
-    rim_send[0] = ext[rows : rows + RIM, :].astype(bf16)
-    rim_send[1] = ext[RIM : 2 * RIM, :].astype(bf16)
     up_rim = ep_copy(rim_send.at[0], rim_recv.at[0], rim_s.at[0], rim_r.at[0], 1)
     down_rim = ep_copy(rim_send.at[1], rim_recv.at[1], rim_s.at[1], rim_r.at[1], ep - 1)
-    up_rim.start()
-    down_rim.start()
-    for load in loads[1:]:
+
+    def enter():
+        for h in range(2):
+            finish(*mixer_part(h))
+        lax.fori_loop(0, rows // chunk, project, 0)
+        rim_send[0] = ext[rows : rows + RIM, :].astype(bf16)
+        rim_send[1] = ext[RIM : 2 * RIM, :].astype(bf16)
+        up_rim.start()
+        down_rim.start()
+
+    for load in loads:
         load.wait()
 
     def hidden_step(k):
@@ -690,9 +735,18 @@
 
     def send_value(k):
         q = ep_from(k)
-        for c, v in enumerate(value_step(k)):
-            back_send[q, c] = v
-        ep_copy(back_send.at[q], back_recv.at[me_ep], bk_s.at[k], bk_r.at[k], ep - k).start()
+        values = value_step(k)
+
+        @pl.when(k > 0)
+        def _():
+            for c in range(2):
+                back_send[q, c] = values[c]
+            ep_copy(back_send.at[q], back_recv.at[me_ep], bk_s.at[k], bk_r.at[k], ep - k).start()
+
+        @pl.when(k == 0)
+        def _():
+            for c in range(2):
+                back_recv[me_ep, c] = values[c]
 
     def combine(e):
         slot = lax.broadcasted_iota(jnp.int32, (rows, cap), 1) + e * cap
@@ -710,7 +764,11 @@
 
     def gather_value(k):
         e = lax.rem(me_ep + k, ep)
-        ep_copy(back_send.at[e], back_recv.at[e], bk_s.at[k], bk_r.at[k], k).wait_recv()
+
+        @pl.when(k > 0)
+        def _():
+            ep_copy(back_send.at[e], back_recv.at[e], bk_s.at[k], bk_r.at[k], k).wait_recv()
+
         combine(e)
 
     def pool():
@@ -743,84 +801,97 @@
             pooled[me_tp, i * chunk : (i + 1) * chunk, :] = (
                 (result - values) * scale[...]
             ).astype(bf16)
-        send(*pooled_part())
+        for h in range(2):
+            send(*pooled_part(h))
 
     acc[...] = jnp.zeros_like(acc)
 
-    def step(i, carry):
-        @pl.when(i + AHEAD + 1 < ep)
-        def _():
-            arrive(lax.rem(i + AHEAD + 1, ep))
-
-        @pl.when(i + AHEAD + 1 == ep)
-        def _():
-            send(*slot_part(0))
-
-        @pl.when(i + 1 < ep)
-        def _():
-            relay(*slot_part(lax.rem(i + 2, ep)), 1)
-
-        hidden_step(lax.rem(i + 1, ep))
-
-        @pl.when(i == POOL_AT)
-        def _():
-            pool()
-
-        @pl.when(i == 0)
-        def _():
-            for r in range(2):
-                down_copy(r).wait_recv()
-
-        @pl.when(i > 0)
-        def _():
-            send_value(i)
-
-        @pl.when(i > BEHIND)
-        def _():
-            gather_value(i - BEHIND)
-
-        return carry
-
-    lax.fori_loop(0, ep, step, 0)
-    relay(*pooled_part(), 0)
-    for c, v in enumerate(value_step(0)):
-        back_recv[me_ep, c] = v
-    combine(me_ep)
-
-    def rest(k, carry):
-        gather_value(k)
-        return carry
-
-    lax.fori_loop(ep - BEHIND, ep, rest, 0)
-    fin_send[...] = acc[1 - col].astype(bf16)
     final = tp_copy(fin_send, fin_recv, fi_s.at[0], fi_r.at[0], beside)
-    final.start()
-
-    finish(*pooled_part())
-
-    def mix_out(i, carry):
-        at = pl.ds(pl.multiple_of(i * chunk, chunk), chunk)
-        total = jnp.zeros((chunk, chan), f32)
-        for p in range(tp):
-            total = total + jnp.dot(
-                pooled[p, at, :],
-                w_mix[p * chan : (p + 1) * chan, :],
-                preferred_element_type=f32,
-            )
-        out_m[at, :] = total.astype(bf16)
-        return carry
-
-    lax.fori_loop(0, rows // chunk, mix_out, 0)
+
+    def exchange(k):
+        fin_send[...] = acc[1 - col].astype(bf16)
+        final.start()
+
+    def mix_out(h):
+        finish(*pooled_part(h))
+
+        def mix(i, carry):
+            at = pl.ds(pl.multiple_of(h * (rows // 2) + i * chunk, chunk), chunk)
+            total = jnp.zeros((chunk, chan), f32)
+            for p in range(tp):
+                total = total + jnp.dot(
+                    pooled[p, at, :],
+                    w_mix[p * chan : (p + 1) * chan, :],
+                    preferred_element_type=f32,
+                )
+            out_m[at, :] = total.astype(bf16)
+            return carry
+
+        lax.fori_loop(0, rows // 2 // chunk, mix, 0)
+
+    def await_down():
+        for i in range(4):
+            down_copy(i).wait_recv()
+
+    body = dict(
+        starts,
+        A=arrive,
+        H=hidden_step,
+        V=send_value,
+        G=gather_value,
+        ENT=lambda k: enter(),
+        POOL=lambda k: pool(),
+        EX=exchange,
+        MIX=mix_out,
+    )
+    turned = {
+        "R": lambda k, turn: relay(*slot_part(k), turn),
+        "RXM": lambda k, turn: relay(*mixer_part(k), turn),
+        "RPO": lambda k, turn: relay(*pooled_part(k), turn),
+    }
+
+    steps = [[]]
+    for op, k in ORDER[picks_at + 1 :]:
+        if steps[-1] and PLACES.index(op) <= PLACES.index(steps[-1][-1][0]):
+            steps.append([])
+        steps[-1].append((op, k))
+    where = {op: [] for op in PLACES}
+    for n, entries in enumerate(steps):
+        for op, k in entries:
+            where[op].append((n, k))
+
+    def step(n, carry):
+        for op in PLACES:
+            spots = where[op]
+            if not spots:
+                continue
+            due = functools.reduce(jnp.logical_or, [n == i for i, _ in spots])
+            k = sum(jnp.where(n == i, v, 0) for i, v in spots)
+
+            @pl.when(due)
+            def _(op=op, k=k, spots=spots):
+                if op == "V":
+                    pl.when(n == spots[0][0])(await_down)
+                if op in turned:
+                    ups = [i for i, v in spots if (op, v) in OVER_X]
+                    turned[op](k, sum(jnp.where(n == i, 1, 0) for i in ups) if ups else 0)
+                else:
+                    body[op](k)
+
+        return carry
+
+    lax.fori_loop(0, len(steps), step, 0)
     final.wait_recv()
     out_e[...] = (acc[col] + fin_recv[...].astype(f32)).astype(bf16)
 
     final.wait_send()
-    drain(*mixer_part())
-    drain(*pooled_part())
+    for h in range(2):
+        drain(*mixer_part(h))
+        drain(*pooled_part(h))
     up_rim.wait_send()
     down_rim.wait_send()
-    for r in range(2):
-        down_copy(r).wait_send()
+    for i in range(4):
+        down_copy(i).wait_send()
 
     def drain_ep(k, carry):
         e = lax.rem(me_ep + k, ep)
@@ -869,20 +940,20 @@
         dma((7,)),
         dma((ep, 3)),
         dma((ep, 3)),
-        dma((3,)),
-        dma((3,)),
+        dma((2, 3)),
+        dma((2, 3)),
         dma((ep,)),
         dma((ep,)),
         dma((2,)),
         dma((2,)),
-        dma((3,)),
-        dma((3,)),
+        dma((2, 3)),
+        dma((2, 3)),
         dma((ep,)),
         dma((ep,)),
         dma((ep,)),
         dma((ep,)),
-        dma((2,)),
-        dma((2,)),
+        dma((4,)),
+        dma((4,)),
         dma((1,)),
         dma((1,)),
     ]
@@ -913,7 +984,7 @@
     vmem = pl.BlockSpec(memory_space=pltpu.VMEM)
     hbm = pl.BlockSpec(memory_space=pl.ANY)
     dma = pltpu.SemaphoreType.DMA
-    square_ok = tp == 4 and ep > AHEAD + 1
+    square_ok = tp == 4 and ep == len(SENDS) + 1
     whole_scratch = [
         pltpu.VMEM(w_in.shape, bf16),
         pltpu.VMEM(w_mix_out.shape, bf16),

time: 160 us -> 148 us (0.925)
  the two profiles are of different devices: /device:TPU:0 before, /device:TPU:9 now
where the time goes in v2:
time: 148 us
  Pallas kernels  144 us (97%)
  local copies, waits for them, and re-layouts  3.74 us (3%)
    pallas_call x1, Pallas kernels, on_device(): pl.pallas_call(functools.partial(square if square_ok else fused, ep, tp),...  144 us
    unnamed x2, local copies, waits for them, and re-layouts  3.74 us

profile of v2, /device:TPU:9, one launch (start us, length us, event | category | flops | bytes accessed | tf_op | source)
XLA Modules:
  0.0 147.9 jit_solution(8981756352149311464)
XLA Ops:
  0.6 143.5 %shard_map.131 = (bf16[512,512]{1,0:T(8,128)(2,1)}, bf16[512,512]{1,0:T(8,128)(2,1)}) custom-call(bf16[512,512]{1,0:T(8,128)(2,1)} %xm_in.1, bf16[512,512]{1,0:T(8,128)(2,1)} %xe_in.1, f32[1,2048]{1,0:T(1,128)} %bitcast.11, f32[1,2048]{1,0:T(1,128)} %bitcast.12, f32[1,512]{1,0:T(1,128)} %bitcast.15, s32[2,512]{1,0:T(2,128)} %bitcast.13, f32[2,512]{1,0:T(2,128)} %bitcast.14, ...), custom_call_target="tpu_custom_call" | custom-call | tf_op jit(solution)/shard_map/pallas_call | solution.py:1029
  144.2 1.9 %copy.16 = bf16[512,512]{1,0:T(8,128)(2,1)} copy(bf16[512,512]{1,0:T(8,128)(2,1)} %get-tuple-element.4) | data formatting | bytes 1048576
  146.0 1.9 %copy.17 = bf16[512,512]{1,0:T(8,128)(2,1)} copy(bf16[512,512]{1,0:T(8,128)(2,1)} %get-tuple-element.5) | data formatting | bytes 1048576

commit v3 on v2

--- a/solution.py
+++ b/solution.py
@@ -12,26 +12,26 @@
 pool_windows = (2, 4, 8, 16)
 RIM = 16
 ORDER = (
-    ("W", 1), ("XMY", 1), ("P", -1), ("XMY", 0), ("W", 2), ("A", 6),
-    ("W", 3), ("A", 2), ("A", 7), ("W", 0), ("R", 6), ("R", 2),
-    ("R", 7), ("H", 6), ("A", 3), ("A", 1), ("H", 7), ("R", 3),
-    ("H", 2), ("V", 6), ("A", 4), ("H", 3), ("R", 1), ("XMX", 1),
-    ("V", 7), ("V", 2), ("R", 4), ("A", 5), ("XMX", 0), ("H", 4),
-    ("A", 0), ("V", 3), ("R", 5), ("RXM", 1), ("V", 4), ("H", 1),
-    ("R", 0), ("G", 6), ("RXM", 0), ("H", 5), ("V", 1), ("ENT", -1),
-    ("H", 0), ("POOL", -1), ("V", 5), ("V", 0), ("G", 3), ("G", 7),
-    ("G", 0), ("G", 1), ("G", 2), ("G", 4), ("RPO", 0), ("G", 5),
-    ("RPO", 1), ("EX", -1), ("MIX", 0), ("MIX", 1),
+    ("XMY", 0), ("W", 2), ("W", 1), ("P", -1), ("XMY", 1), ("A", 0),
+    ("A", 3), ("A", 4), ("R", 0), ("R", 3), ("R", 4), ("W", 0),
+    ("W", 3), ("H", 3), ("H", 4), ("XMX", 0), ("A", 1), ("A", 5),
+    ("A", 6), ("A", 2), ("V", 3), ("XMX", 1), ("V", 4), ("R", 5),
+    ("R", 6), ("H", 5), ("A", 7), ("R", 2), ("R", 1), ("V", 5),
+    ("H", 6), ("G", 4), ("RXM", 1), ("H", 2), ("RXM", 0), ("H", 0),
+    ("V", 6), ("R", 7), ("G", 5), ("H", 1), ("ENT", -1), ("V", 2),
+    ("H", 7), ("G", 3), ("POOL", -1), ("V", 1), ("V", 0), ("G", 0),
+    ("G", 6), ("G", 2), ("V", 7), ("G", 7), ("G", 1), ("EX", -1),
+    ("RPO", 0), ("RPO", 1), ("MIX", 0), ("MIX", 1),
 )
 SENDS = (
-    6, 2, 7, 3, 4, 1, 5,
+    3, 4, 1, 6, 5, 2, 7,
 )
 OVER_X = (
-    ("R", 0), ("R", 3), ("R", 4), ("R", 5), ("R", 7), ("RXM", 1),
+    ("R", 0), ("R", 2), ("R", 7), ("RXM", 0), ("RXM", 1),
 )
 PLACES = (
-    "ENT", "XMY", "W", "R", "G", "RXM", "A", "RPO",
-    "XMX", "H", "EX", "POOL", "MIX", "V",
+    "W", "RXM", "POOL", "H", "XMY", "XMX", "A", "ENT",
+    "V", "R", "G", "EX", "RPO", "MIX",
 )
 MESH = pl.DeviceIdType.MESH
 f32 = jnp.float32
@@ -502,6 +502,8 @@
     width = feat * tp
     chunk = min(rows, 128)
 
+    not_first = me_ep > 0
+    not_last = me_ep < ep - 1
     col = lax.rem(me_tp, 2)
     row = me_tp // 2
     beside = row * 2 + (1 - col)
@@ -705,8 +707,8 @@
         lax.fori_loop(0, rows // chunk, project, 0)
         rim_send[0] = ext[rows : rows + RIM, :].astype(bf16)
         rim_send[1] = ext[RIM : 2 * RIM, :].astype(bf16)
-        up_rim.start()
-        down_rim.start()
+        pl.when(not_last)(up_rim.start)
+        pl.when(not_first)(down_rim.start)
 
     for load in loads:
         load.wait()
@@ -772,12 +774,19 @@
         combine(e)
 
     def pool():
-        up_rim.wait_recv()
-        down_rim.wait_recv()
-        low = rim_recv[0].astype(f32)
-        high = rim_recv[1].astype(f32)
-        ext[0:RIM, :] = jnp.where(me_ep > 0, low, 0.0)
-        ext[RIM + rows : 2 * RIM + rows, :] = jnp.where(me_ep < ep - 1, high, 0.0)
+        ext[0:RIM, :] = jnp.zeros((RIM, chan), f32)
+        ext[RIM + rows : 2 * RIM + rows, :] = jnp.zeros((RIM, chan), f32)
+
+        @pl.when(not_first)
+        def _():
+            up_rim.wait_recv()
+            ext[0:RIM, :] = rim_recv[0].astype(f32)
+
+        @pl.when(not_last)
+        def _():
+            down_rim.wait_recv()
+            ext[RIM + rows : 2 * RIM + rows, :] = rim_recv[1].astype(f32)
+
         group_width = chan * tp // len(pool_windows)
         channel = me_tp * chan + lax.broadcasted_iota(jnp.int32, (1, chan), 1)
         seq_len = rows * ep
@@ -888,8 +897,8 @@
     for h in range(2):
         drain(*mixer_part(h))
         drain(*pooled_part(h))
-    up_rim.wait_send()
-    down_rim.wait_send()
+    pl.when(not_last)(up_rim.wait_send)
+    pl.when(not_first)(down_rim.wait_send)
     for i in range(4):
         down_copy(i).wait_send()
 
@@ -957,6 +966,11 @@
         dma((1,)),
         dma((1,)),
     ]
+
+
+def hand_over(m_in, e_in, m_out, e_out):
+    m_out[...] = m_in[...]
+    e_out[...] = e_in[...]
 
 
 def on_device(
@@ -1026,7 +1040,7 @@
         shapes = (w_in.shape, w_mix_out.shape, expert_gate.shape[1:], expert_up.shape[1:])
         cols = expert_down.shape[2]
         whole_scratch = square_scratch(ep, tp, rows, feat, cap, chan, units, cols, shapes)
-    return pl.pallas_call(
+    result = pl.pallas_call(
         functools.partial(square if square_ok else fused, ep, tp),
         out_shape=(
             jax.ShapeDtypeStruct((rows, w_mix_out.shape[1]), bf16),
@@ -1052,6 +1066,14 @@
         expert_up.reshape(expert_up.shape[1:]),
         expert_down.reshape(expert_down.shape[1:]),
     )
+    if not square_ok:
+        return result
+    return pl.pallas_call(
+        hand_over,
+        out_shape=tuple(jax.ShapeDtypeStruct(v.shape, v.dtype) for v in result),
+        in_specs=[vmem, vmem],
+        out_specs=(vmem, vmem),
+    )(*result)
 
 
 def solution(mesh):

time: 148 us -> 142 us (0.959)
  the two profiles are of different devices: /device:TPU:9 before, /device:TPU:0 now
where the time goes in v3:
time: 142 us; the launch traced here: 141 us
  Pallas kernels  141 us (99%)
    pallas_call x1, Pallas kernels, on_device(): pl.pallas_call(functools.partial(square if square_ok else fused, ep, tp),...  139 us

profile of v3, /device:TPU:0, one launch (start us, length us, event | category | flops | bytes accessed | tf_op | source)
XLA Modules:
  0.0 141.4 jit_solution(7917582286800054116)
XLA Ops:
  0.6 138.6 %shard_map.131 = (bf16[512,512]{1,0:T(8,128)(2,1)}, bf16[512,512]{1,0:T(8,128)(2,1)}) custom-call(bf16[512,512]{1,0:T(8,128)(2,1)} %xm_in.1, bf16[512,512]{1,0:T(8,128)(2,1)} %xe_in.1, f32[1,2048]{1,0:T(1,128)} %bitcast.11, f32[1,2048]{1,0:T(1,128)} %bitcast.12, f32[1,512]{1,0:T(1,128)} %bitcast.15, s32[2,512]{1,0:T(2,128)} %bitcast.13, f32[2,512]{1,0:T(2,128)} %bitcast.14, ...), custom_call_target="tpu_custom_call" | custom-call | tf_op jit(solution)/shard_map/pallas_call | solution.py:1043
  139.2 2.2 %shard_map.132 = (bf16[512,512]{1,0:T(8,128)(2,1)}, bf16[512,512]{1,0:T(8,128)(2,1)}) custom-call(bf16[512,512]{1,0:T(8,128)(2,1)} %get-tuple-element.4.m_in, bf16[512,512]{1,0:T(8,128)(2,1)} %get-tuple-element.5.e_in), custom_call_target="tpu_custom_call" | custom-call | tf_op jit(solution)/shard_map/pallas_call | solution.py:1071

commit v4 on v3

--- a/solution.py
+++ b/solution.py
@@ -12,26 +12,27 @@
 pool_windows = (2, 4, 8, 16)
 RIM = 16
 ORDER = (
-    ("XMY", 0), ("W", 2), ("W", 1), ("P", -1), ("XMY", 1), ("A", 0),
-    ("A", 3), ("A", 4), ("R", 0), ("R", 3), ("R", 4), ("W", 0),
-    ("W", 3), ("H", 3), ("H", 4), ("XMX", 0), ("A", 1), ("A", 5),
-    ("A", 6), ("A", 2), ("V", 3), ("XMX", 1), ("V", 4), ("R", 5),
-    ("R", 6), ("H", 5), ("A", 7), ("R", 2), ("R", 1), ("V", 5),
-    ("H", 6), ("G", 4), ("RXM", 1), ("H", 2), ("RXM", 0), ("H", 0),
-    ("V", 6), ("R", 7), ("G", 5), ("H", 1), ("ENT", -1), ("V", 2),
-    ("H", 7), ("G", 3), ("POOL", -1), ("V", 1), ("V", 0), ("G", 0),
-    ("G", 6), ("G", 2), ("V", 7), ("G", 7), ("G", 1), ("EX", -1),
-    ("RPO", 0), ("RPO", 1), ("MIX", 0), ("MIX", 1),
+    ("XMY", 1), ("W", 2), ("P", -1), ("W", 3), ("A", 0), ("XMY", 0),
+    ("A", 2), ("A", 4), ("R", 2), ("R", 4), ("W", 1), ("A", 3),
+    ("H", 2), ("W", 0), ("H", 4), ("A", 6), ("R", 3), ("A", 7),
+    ("V", 2), ("R", 0), ("A", 5), ("G", 2), ("V", 4), ("H", 3),
+    ("R", 6), ("XMX", 0), ("R", 5), ("V", 3), ("H", 0), ("XMX", 1),
+    ("R", 7), ("H", 5), ("RXM", 1), ("RXM", 0), ("V", 5), ("G", 4),
+    ("V", 0), ("A", 1), ("H", 7), ("G", 0), ("ENT", -1), ("H", 6),
+    ("R", 1), ("V", 7), ("H", 1), ("V", 6), ("POOL", -1), ("G", 3),
+    ("V", 1), ("G", 7), ("G", 1), ("G", 5), ("RPO", 0), ("G", 6),
+    ("EX", -1), ("RPO", 1), ("MIX", 0), ("MIX", 1),
 )
 SENDS = (
-    3, 4, 1, 6, 5, 2, 7,
+    2, 4, 1, 3, 7, 6, 5,
 )
 OVER_X = (
-    ("R", 0), ("R", 2), ("R", 7), ("RXM", 0), ("RXM", 1),
+    ("R", 0, 0), ("R", 1, 0), ("R", 1, 1), ("R", 2, 0), ("R", 3, 1), ("R", 5, 0),
+    ("R", 5, 1), ("R", 7, 0), ("R", 7, 1), ("RXM", 1, 0),
 )
 PLACES = (
-    "W", "RXM", "POOL", "H", "XMY", "XMX", "A", "ENT",
-    "V", "R", "G", "EX", "RPO", "MIX",
+    "W", "POOL", "A", "H", "G", "XMX", "R", "RXM",
+    "V", "EX", "RPO", "ENT", "XMY", "MIX",
 )
 MESH = pl.DeviceIdType.MESH
 f32 = jnp.float32
@@ -437,17 +438,25 @@
     ep,
     tp,
     xm_in,
+    xe_h,
+    gain_m_h,
+    gain_e_h,
+    scale_h,
+    routes_h,
+    rw_h,
+    w_in_h,
+    w_mix_h,
+    gate_h,
+    up_h,
+    down_h,
+    out_m_h,
+    out_e_h,
     xe_in,
     gain_m,
     gain_e,
     scale,
     route_rows,
     rw_rows,
-    w_in_h,
-    w_mix_h,
-    gate_h,
-    up_h,
-    down_h,
     out_m,
     out_e,
     w_in,
@@ -472,6 +481,8 @@
     fin_recv,
     as_rows,
     as_cols,
+    in_sem,
+    out_sem,
     w_sem,
     sl_s,
     sl_r,
@@ -520,6 +531,21 @@
             barrier, inc=1, device_id={"ep": lax.rem(me_ep + d, ep)}, device_id_type=MESH
         )
 
+    inputs = [
+        pltpu.make_async_copy(h, v, in_sem.at[i])
+        for i, (h, v) in enumerate(
+            (
+                (routes_h, route_rows),
+                (rw_h, rw_rows),
+                (xe_h, xe_in),
+                (gain_m_h, gain_m),
+                (gain_e_h, gain_e),
+                (scale_h, scale),
+            )
+        )
+    ]
+    for load in inputs:
+        load.start()
     xm_load = pltpu.make_async_copy(xm_in, xm.at[me_tp], w_sem.at[0])
     xm_load.start()
 
@@ -541,9 +567,6 @@
             )
         )
     ]
-    for load in loads:
-        load.start()
-
     def tp_copy(src, dst, s, r, peer):
         return pltpu.make_async_remote_copy(
             src_ref=src,
@@ -586,6 +609,34 @@
     def half_rows(h):
         return pl.ds(pl.multiple_of(h * (rows // 2), rows // 2), rows // 2)
 
+    part = cap // 2
+
+    def slot_half(k, p, h):
+        return slots.at[ep_from(k), p, pl.ds(h * part, part)]
+
+    def relay_slot(k, turns):
+        slot, s, r = slot_part(k)
+        tp_copy(slot(beside), slot(beside), s(0), r(0), beside).wait_recv()
+        tp_copy(slot(above), slot(above), s(1), r(1), above).wait_recv()
+        for h, turn in enumerate(turns):
+            source = slot_half(k, (1 - turn) * beside + turn * above, h)
+            peer = (1 - turn) * above + turn * beside
+            tp_copy(source, source, s(2 + h), r(2 + h), peer).start()
+
+    def finish_slot(k):
+        slot, s, r = slot_part(k)
+        for h in range(2):
+            source = slot_half(k, across, h)
+            tp_copy(source, source, s(2 + h), r(2 + h), across).wait_recv()
+
+    def drain_slot(k):
+        slot, s, r = slot_part(k)
+        for j in range(2):
+            tp_copy(slot(me_tp), slot(me_tp), s(j), r(j), beside).wait_send()
+        for h in range(2):
+            source = slot_half(k, across, h)
+            tp_copy(source, source, s(2 + h), r(2 + h), beside).wait_send()
+
     def mixer_part(h):
         at = half_rows(h)
         return lambda p: xm.at[p, at], lambda j: xm_s.at[h, j], lambda j: xm_r.at[h, j]
@@ -606,11 +657,11 @@
         return tp_copy(ref, ref, hi_s.at[k], hi_r.at[k], above)
 
     def down_copy(i):
-        r, part = i // 2, i % 2
-        first = (r * 2 + 1 - col) * units + part * piece
+        r, half = i // 2, i % 2
+        first = (r * 2 + 1 - col) * units + half * piece
         return tp_copy(
             down_h.at[pl.ds(pl.multiple_of(first, piece), piece), :],
-            down.at[col, r, pl.ds(pl.multiple_of(part * piece, piece), piece)],
+            down.at[col, r, pl.ds(pl.multiple_of(half * piece, piece), piece)],
             dn_s.at[i],
             dn_r.at[i],
             beside,
@@ -624,6 +675,8 @@
         slot, s, r = mixer_part(h)
         tp_copy(slot(me_tp), slot(me_tp), s(1), r(1), above).start()
 
+    for load in inputs[:2]:
+        load.wait()
     t0 = lax.broadcasted_iota(jnp.int32, (rows, rows), 0)
     t1 = lax.broadcasted_iota(jnp.int32, (rows, rows), 1)
     names = lax.broadcasted_iota(jnp.int32, (ep, rows), 0)
@@ -644,7 +697,11 @@
         as_rows[TOP + j : TOP + j + 1, :] = rw_rows[j : j + 1, :]
     as_cols[...] = as_rows[...].T
 
+    for load in inputs[2:]:
+        load.wait()
     xm_load.wait()
+    for load in loads:
+        load.start()
     pl.semaphore_wait(barrier, tp + ep - 2)
     starts = {
         "W": lambda k: down_copy(k).start(),
@@ -715,7 +772,7 @@
 
     def hidden_step(k):
         q = ep_from(k)
-        finish(*slot_part(k))
+        finish_slot(k)
         for p, v in enumerate(norm_rows([slots[q, p] for p in range(tp)], gain_e)):
             block[:, p * feat : (p + 1) * feat] = v
         x = block[...]
@@ -752,17 +809,16 @@
 
     def combine(e):
         slot = lax.broadcasted_iota(jnp.int32, (rows, cap), 1) + e * cap
-        weight = jnp.zeros((rows, cap), f32)
+        hit = None
+        weight = jnp.zeros((rows, 1), f32)
         for j in range(TOP):
             own_slot = as_cols[:, j : j + 1].astype(jnp.int32)
-            weight = weight + jnp.where(slot == own_slot, as_cols[:, TOP + j : TOP + j + 1], 0.0)
-        coarse = weight.astype(bf16)
-        fine = (weight - coarse.astype(f32)).astype(bf16)
+            here = (own_slot >= e * cap) & (own_slot < (e + 1) * cap)
+            weight = weight + jnp.where(here, as_cols[:, TOP + j : TOP + j + 1], 0.0)
+            hit = slot == own_slot if hit is None else hit | (slot == own_slot)
+        pick = jnp.where(hit, 1.0, 0.0).astype(bf16)
         for c in range(2):
-            v = back_recv[e, c]
-            acc[c] += jnp.dot(coarse, v, preferred_element_type=f32) + jnp.dot(
-                fine, v, preferred_element_type=f32
-            )
+            acc[c] += weight * jnp.dot(pick, back_recv[e, c], preferred_element_type=f32)
 
     def gather_value(k):
         e = lax.rem(me_ep + k, ep)
@@ -821,6 +877,10 @@
         fin_send[...] = acc[1 - col].astype(bf16)
         final.start()
 
+    def mixed_out(h):
+        at = half_rows(h)
+        return pltpu.make_async_copy(out_m.at[at], out_m_h.at[at], out_sem.at[h])
+
     def mix_out(h):
         finish(*pooled_part(h))
 
@@ -837,6 +897,7 @@
             return carry
 
         lax.fori_loop(0, rows // 2 // chunk, mix, 0)
+        mixed_out(h).start()
 
     def await_down():
         for i in range(4):
@@ -854,9 +915,9 @@
         MIX=mix_out,
     )
     turned = {
-        "R": lambda k, turn: relay(*slot_part(k), turn),
-        "RXM": lambda k, turn: relay(*mixer_part(k), turn),
-        "RPO": lambda k, turn: relay(*pooled_part(k), turn),
+        "R": lambda k, turns: relay_slot(k, turns),
+        "RXM": lambda k, turns: relay(*mixer_part(k), turns[0]),
+        "RPO": lambda k, turns: relay(*pooled_part(k), turns[0]),
     }
 
     steps = [[]]
@@ -882,8 +943,11 @@
                 if op == "V":
                     pl.when(n == spots[0][0])(await_down)
                 if op in turned:
-                    ups = [i for i, v in spots if (op, v) in OVER_X]
-                    turned[op](k, sum(jnp.where(n == i, 1, 0) for i in ups) if ups else 0)
+                    turns = []
+                    for h in range(2):
+                        ups = [i for i, v in spots if (op, v, h) in OVER_X]
+                        turns.append(sum(jnp.where(n == i, 1, 0) for i in ups) if ups else 0)
+                    turned[op](k, turns)
                 else:
                     body[op](k)
 
@@ -892,6 +956,8 @@
     lax.fori_loop(0, len(steps), step, 0)
     final.wait_recv()
     out_e[...] = (acc[col] + fin_recv[...].astype(f32)).astype(bf16)
+    last = pltpu.make_async_copy(out_e, out_e_h, out_sem.at[2])
+    last.start()
 
     final.wait_send()
     for h in range(2):
@@ -912,11 +978,14 @@
     lax.fori_loop(1, ep, drain_ep, 0)
 
     def drain_tp(k, carry):
-        drain(*slot_part(k))
+        drain_slot(k)
         hidden_copy(k, row).wait_send()
         return carry
 
     lax.fori_loop(0, ep, drain_tp, 0)
+    for h in range(2):
+        mixed_out(h).wait()
+    last.wait()
 
 
 def square_scratch(ep, tp, rows, feat, cap, chan, units, cols, shapes):
@@ -924,6 +993,14 @@
     width = feat * tp
     w_in, w_mix, gate, up = shapes
     return [
+        pltpu.VMEM((rows, feat), bf16),
+        pltpu.VMEM((1, width), f32),
+        pltpu.VMEM((1, width), f32),
+        pltpu.VMEM((1, chan), f32),
+        pltpu.VMEM((TOP, rows), jnp.int32),
+        pltpu.VMEM((TOP, rows), f32),
+        pltpu.VMEM((rows, chan), bf16),
+        pltpu.VMEM((rows, cols), bf16),
         pltpu.VMEM(w_in, bf16),
         pltpu.VMEM(w_mix, bf16),
         pltpu.VMEM(gate, bf16),
@@ -946,9 +1023,11 @@
         pltpu.VMEM((rows, cols), bf16),
         pltpu.VMEM((8, rows), f32),
         pltpu.VMEM((rows, 8), f32),
+        dma((6,)),
+        dma((3,)),
         dma((7,)),
-        dma((ep, 3)),
-        dma((ep, 3)),
+        dma((ep, 4)),
+        dma((ep, 4)),
         dma((2, 3)),
         dma((2, 3)),
         dma((ep,)),
@@ -968,9 +1047,22 @@
     ]
 
 
-def hand_over(m_in, e_in, m_out, e_out):
-    m_out[...] = m_in[...]
-    e_out[...] = e_in[...]
+def hand_over(m_in, e_in, m_out, e_out, held, sem):
+    pieces = held.shape[1]
+    rows = held.shape[2]
+    ways = []
+    for i, (src, dst) in enumerate(((m_in, m_out), (e_in, e_out))):
+        for j in range(pieces):
+            at = pl.ds(j * rows, rows)
+            into = pltpu.make_async_copy(src.at[at], held.at[i, j], sem.at[0, i, j])
+            into.start()
+            out = pltpu.make_async_copy(held.at[i, j], dst.at[at], sem.at[1, i, j])
+            ways.append((into, out))
+    for into, out in ways:
+        into.wait()
+        out.start()
+    for _, out in ways:
+        out.wait()
 
 
 def on_device(
@@ -1046,8 +1138,8 @@
             jax.ShapeDtypeStruct((rows, w_mix_out.shape[1]), bf16),
             jax.ShapeDtypeStruct((rows, expert_down.shape[2]), bf16),
         ),
-        in_specs=[hbm if square_ok else vmem] + [vmem] * 6 + [hbm] * 5,
-        out_specs=(vmem, vmem),
+        in_specs=[hbm if square_ok else vmem] * 7 + [hbm] * 5,
+        out_specs=(hbm, hbm) if square_ok else (vmem, vmem),
         scratch_shapes=whole_scratch,
         compiler_params=pltpu.CompilerParams(
             collective_id=0, has_side_effects=True, vmem_limit_bytes=62 * 1024 * 1024
@@ -1068,11 +1160,16 @@
     )
     if not square_ok:
         return result
+    pieces = 2
     return pl.pallas_call(
         hand_over,
         out_shape=tuple(jax.ShapeDtypeStruct(v.shape, v.dtype) for v in result),
-        in_specs=[vmem, vmem],
-        out_specs=(vmem, vmem),
+        in_specs=[hbm, hbm],
+        out_specs=(hbm, hbm),
+        scratch_shapes=[
+            pltpu.VMEM((2, pieces, rows // pieces, cols), bf16),
+            pltpu.SemaphoreType.DMA((2, 2, pieces)),
+        ],
     )(*result)
 
 

time: 142 us -> 137 us (0.965)
  the two profiles are of different devices: /device:TPU:0 before, /device:TPU:27 now
where the time goes in v4:
time: 137 us
  Pallas kernels  136 us (99%)
    pallas_call x1, Pallas kernels, on_device(): pl.pallas_call(functools.partial(square if square_ok else fused, ep, tp),...  134 us

profile of v4, /device:TPU:27, one launch (start us, length us, event | category | flops | bytes accessed | tf_op | source)
XLA Modules:
  0.0 137.0 jit_solution(11357527018012991106)
XLA Ops:
  0.6 134.4 %shard_map.131 = (bf16[512,512]{1,0:T(8,128)(2,1)}, bf16[512,512]{1,0:T(8,128)(2,1)}) custom-call(bf16[512,512]{1,0:T(8,128)(2,1)} %xm_in.1, bf16[512,512]{1,0:T(8,128)(2,1)} %xe_h.1, f32[1,2048]{1,0:T(1,128)} %bitcast.11, f32[1,2048]{1,0:T(1,128)} %bitcast.12, f32[1,512]{1,0:T(1,128)} %bitcast.15, s32[2,512]{1,0:T(2,128)} %bitcast.13, f32[2,512]{1,0:T(2,128)} %bitcast.14, ...), custom_call_target="tpu_custom_call" | custom-call | tf_op jit(solution)/shard_map/pallas_call | solution.py:1135
  135.0 2.0 %shard_map.132 = (bf16[512,512]{1,0:T(8,128)(2,1)}, bf16[512,512]{1,0:T(8,128)(2,1)}) custom-call(bf16[512,512]{1,0:T(8,128)(2,1)} %get-tuple-element.4.m_in, bf16[512,512]{1,0:T(8,128)(2,1)} %get-tuple-element.5.e_in), custom_call_target="tpu_custom_call" | custom-call | tf_op jit(solution)/shard_map/pallas_call | solution.py:1164

commit v5 on v4

--- a/solution.py
+++ b/solution.py
@@ -18,9 +18,9 @@
     ("V", 2), ("R", 0), ("A", 5), ("G", 2), ("V", 4), ("H", 3),
     ("R", 6), ("XMX", 0), ("R", 5), ("V", 3), ("H", 0), ("XMX", 1),
     ("R", 7), ("H", 5), ("RXM", 1), ("RXM", 0), ("V", 5), ("G", 4),
-    ("V", 0), ("A", 1), ("H", 7), ("G", 0), ("ENT", -1), ("H", 6),
-    ("R", 1), ("V", 7), ("H", 1), ("V", 6), ("POOL", -1), ("G", 3),
-    ("V", 1), ("G", 7), ("G", 1), ("G", 5), ("RPO", 0), ("G", 6),
+    ("V", 0), ("A", 1), ("H", 7), ("G", 0), ("ENT", -1), ("R", 1),
+    ("H", 6), ("V", 7), ("H", 1), ("V", 6), ("POOL", -1), ("G", 3),
+    ("G", 5), ("V", 1), ("G", 7), ("G", 1), ("RPO", 0), ("G", 6),
     ("EX", -1), ("RPO", 1), ("MIX", 0), ("MIX", 1),
 )
 SENDS = (
@@ -31,8 +31,8 @@
     ("R", 5, 1), ("R", 7, 0), ("R", 7, 1), ("RXM", 1, 0),
 )
 PLACES = (
-    "W", "POOL", "A", "H", "G", "XMX", "R", "RXM",
-    "V", "EX", "RPO", "ENT", "XMY", "MIX",
+    "W", "A", "POOL", "H", "G", "EX", "XMY", "RPO",
+    "ENT", "RXM", "XMX", "V", "R", "MIX",
 )
 MESH = pl.DeviceIdType.MESH
 f32 = jnp.float32

time: 137 us -> 137 us (level)
  the two profiles are of different devices: /device:TPU:27 before, /device:TPU:24 now
where the time goes in v5:
time: 137 us
  Pallas kernels  136 us (99%)
    pallas_call x1, Pallas kernels, on_device(): pl.pallas_call(functools.partial(square if square_ok else fused, ep, tp),...  134 us

profile of v5, /device:TPU:24, one launch (start us, length us, event | category | flops | bytes accessed | tf_op | source)
XLA Modules:
  0.0 136.7 jit_solution(15298804587324301790)
XLA Ops:
  0.6 134.1 %shard_map.131 = (bf16[512,512]{1,0:T(8,128)(2,1)}, bf16[512,512]{1,0:T(8,128)(2,1)}) custom-call(bf16[512,512]{1,0:T(8,128)(2,1)} %xm_in.1, bf16[512,512]{1,0:T(8,128)(2,1)} %xe_h.1, f32[1,2048]{1,0:T(1,128)} %bitcast.11, f32[1,2048]{1,0:T(1,128)} %bitcast.12, f32[1,512]{1,0:T(1,128)} %bitcast.15, s32[2,512]{1,0:T(2,128)} %bitcast.13, f32[2,512]{1,0:T(2,128)} %bitcast.14, ...), custom_call_target="tpu_custom_call" | custom-call | tf_op jit(solution)/shard_map/pallas_call | solution.py:1135
  134.7 2.0 %shard_map.132 = (bf16[512,512]{1,0:T(8,128)(2,1)}, bf16[512,512]{1,0:T(8,128)(2,1)}) custom-call(bf16[512,512]{1,0:T(8,128)(2,1)} %get-tuple-element.4.m_in, bf16[512,512]{1,0:T(8,128)(2,1)} %get-tuple-element.5.e_in), custom_call_target="tpu_custom_call" | custom-call | tf_op jit(solution)/shard_map/pallas_call | solution.py:1164
